TPU v7x, 32 devices: a whole 2x2x4 slice. The times are simulated.
32 devices in a mesh: sp: 8 (over z, x), tp: 4 (over y, core).
Axes of the slice: x: 2, y: 2, z: 4, core: 2. Of those that a mesh axis runs over, the one named last changes fastest.
Arguments:
- expert_input: bfloat16 [1536, 2048], P('sp'), may hold values from -6 to 6
- norm_gain: float32 [2048], replicated, may hold values from 0.1 to 1.9
- expert_ids: int32 [1536, 2], P('sp'), may hold values from 0 to 7, all different within a row; in each aligned block of 192 rows (0 to 191, 192 to 383, ...) at most 96 rows name the same one
- route_weights: float32 [1536, 2], P('sp'), may hold values from 0.25 to 2.25
- layer_cotangent: bfloat16 [1536, 2048], P('sp'), may hold values from -6 to 6
- gate_weight: bfloat16 [8, 1024, 2048], P('sp', 'tp'), may hold values from -0.125 to 0.125
- up_weight: bfloat16 [8, 1024, 2048], P('sp', 'tp'), may hold values from -0.125 to 0.125
- down_weight: bfloat16 [8, 1024, 2048], P('sp', 'tp'), may hold values from -0.1875 to 0.1875
- proj_b: bfloat16 [1536, 2048], P('sp', 'tp'), may hold values from -6 to 6
- proj_c: bfloat16 [1536, 2048], P('sp', 'tp'), may hold values from -6 to 6
- proj_x: bfloat16 [1536, 2048], P('sp', 'tp'), may hold values from -6 to 6
- conv_taps: float32 [3, 2048], P(None, 'tp'), may hold values from -3 to 3
- out_weight: bfloat16 [2048, 2048], P(None, 'tp'), may hold values from -0.125 to 0.125
Outputs:
- grad_gate: bfloat16 [8, 1024, 2048], P('sp', 'tp')
- grad_up: bfloat16 [8, 1024, 2048], P('sp', 'tp')
- grad_down: bfloat16 [8, 1024, 2048], P('sp', 'tp')
- grad_out_weight: float32 [2048, 2048], P('sp', 'tp')
- grad_b: bfloat16 [1536, 2048], P('sp', 'tp')
- grad_c: bfloat16 [1536, 2048], P('sp', 'tp')
- grad_x: bfloat16 [1536, 2048], P('sp', 'tp')
Inputs may be any that keep to these rules, and one draw needn't show every extreme that they name: `expert_ids`: A token's two experts differ. In the rows of one device each expert is named at most 96 times, a bound that some expert reaches in some blocks.
All inputs are finite; a program needn't handle non-finite values.
Results may differ from a plain program's by a relative error of at most 0.034.
Values may be sent and summed in bfloat16 or wider, within the bound.
A program may use at most 64 MiB of HBM per device.

v0:
```python
import jax
import jax.numpy as jnp
from jax import lax
from jax.sharding import PartitionSpec as P

eps = 1e-06


def passed_along(block, axis, distance):
    devices = range(lax.axis_size(axis))
    route = [(i - distance, i) for i in devices if i - distance in devices]
    return lax.ppermute(block, axis, route)


def slot_layout(routed_flat, experts, capacity):
    pair_count = routed_flat.shape[0]
    onehot = (routed_flat[:, None] == jnp.arange(experts, dtype=jnp.int32)[None, :]).astype(
        jnp.int32
    )
    slot_rank = jnp.sum((jnp.cumsum(onehot, axis=0) - 1) * onehot, axis=1)
    slot_index = routed_flat * capacity + slot_rank
    pair_of = (
        jnp.zeros((experts * capacity,), jnp.int32)
        .at[slot_index]
        .set(jnp.arange(pair_count, dtype=jnp.int32))
    )
    filled = jnp.zeros((experts * capacity,), jnp.int32).at[slot_index].set(1)
    return (slot_index, pair_of, filled)


def on_device(
    expert_input,
    norm_gain,
    expert_ids,
    route_weights,
    layer_cotangent,
    gate_weight,
    up_weight,
    down_weight,
    proj_b,
    proj_c,
    proj_x,
    conv_taps,
    out_weight,
):
    groups = lax.axis_size("sp")
    slices = lax.axis_size("tp")
    tok_rows, model_width = expert_input.shape
    capacity = 4 * tok_rows // groups
    column = model_width // slices
    col_start = lax.axis_index("tp") * column
    layer_in = expert_input.astype(jnp.float32)
    root_mean = jnp.sqrt(jnp.mean(layer_in * layer_in, axis=1, keepdims=True) + eps)
    unit = layer_in / root_mean
    normed = (unit * norm_gain[None, :]).astype(jnp.bfloat16)
    routed_flat = expert_ids.reshape(-1)
    slot_index, pair_of, filled = slot_layout(routed_flat, groups, capacity)
    token_of = pair_of // 2
    filled_mask = (filled > 0)[:, None]
    rows_in = jnp.where(filled_mask, normed[token_of], jnp.zeros((), jnp.bfloat16)).reshape(
        groups, capacity, model_width
    )
    scaled = route_weights.reshape(-1)[pair_of][:, None] * layer_cotangent[token_of].astype(
        jnp.float32
    )
    cots_in = (
        jnp.where(filled_mask, scaled, 0.0)
        .astype(jnp.bfloat16)
        .reshape(groups, capacity, model_width)
    )
    rows_cut = lax.dynamic_slice_in_dim(rows_in, col_start, column, 2)
    cots_cut = lax.dynamic_slice_in_dim(cots_in, col_start, column, 2)
    rows_part, cots_part = (
        lax.all_to_all(rows_cut, "sp", split_axis=0, concat_axis=0, tiled=True),
        lax.all_to_all(cots_cut, "sp", split_axis=0, concat_axis=0, tiled=True),
    )
    rows_at, cots_at = (
        lax.all_gather(rows_part, "tp", axis=2, tiled=True),
        lax.all_gather(cots_part, "tp", axis=2, tiled=True),
    )
    rows_flat = rows_at.reshape(-1, model_width)
    cots_flat = cots_at.reshape(-1, model_width)
    w_gate = gate_weight[0]
    w_up = up_weight[0]
    w_down = down_weight[0]
    contract_last = (((1,), (1,)), ((), ()))
    contract_first = (((0,), (0,)), ((), ()))
    gate_pre = lax.dot_general(rows_flat, w_gate, contract_last, preferred_element_type=jnp.float32)
    up_pre = lax.dot_general(rows_flat, w_up, contract_last, preferred_element_type=jnp.float32)
    grad_hidden = lax.dot_general(
        cots_flat, w_down, contract_last, preferred_element_type=jnp.float32
    )
    sigmoid_gate = jax.nn.sigmoid(gate_pre)
    hidden = (gate_pre * sigmoid_gate * up_pre).astype(jnp.bfloat16)
    down_grad = lax.dot_general(
        hidden, cots_flat, contract_first, preferred_element_type=jnp.float32
    )
    grad_gate_pre = (
        grad_hidden * up_pre * sigmoid_gate * (1.0 + gate_pre * (1.0 - sigmoid_gate))
    ).astype(jnp.bfloat16)
    grad_up_pre = (grad_hidden * gate_pre * sigmoid_gate).astype(jnp.bfloat16)
    gate_grad = lax.dot_general(
        grad_gate_pre, rows_flat, contract_first, preferred_element_type=jnp.float32
    )
    up_grad = lax.dot_general(
        grad_up_pre, rows_flat, contract_first, preferred_element_type=jnp.float32
    )
    partial_value = jnp.dot(grad_gate_pre, w_gate, preferred_element_type=jnp.float32)
    partial_value = partial_value + jnp.dot(grad_up_pre, w_up, preferred_element_type=jnp.float32)
    partial_value = partial_value.reshape(groups, capacity, model_width)
    summed = lax.psum_scatter(
        partial_value.astype(jnp.bfloat16), "tp", scatter_dimension=2, tiled=True
    )
    back = lax.all_to_all(summed, "sp", split_axis=0, concat_axis=0, tiled=True)
    back_flat = back.reshape(groups * capacity, column)
    pairs_grad = back_flat[slot_index].astype(jnp.float32)
    grad_normed = pairs_grad.reshape(tok_rows, 2, column).sum(axis=1)
    unit_cols = lax.dynamic_slice_in_dim(unit, col_start, column, 1)
    gain_cols = lax.dynamic_slice_in_dim(norm_gain, col_start, column, 0)[None, :]
    cot_cols = lax.dynamic_slice_in_dim(layer_cotangent, col_start, column, 1).astype(jnp.float32)
    local_total = jnp.sum(unit_cols * gain_cols * grad_normed, axis=1)
    row_total = lax.psum(local_total, "tp")
    grad_cols = (
        cot_cols
        + (gain_cols * grad_normed - unit_cols * row_total[:, None] / model_width) / root_mean
    )
    grad_cols = grad_cols.astype(jnp.bfloat16)
    grad_input = lax.all_gather(grad_cols, "tp", axis=1, tiled=True)
    tap_first = conv_taps[0][None, :]
    tap_middle = conv_taps[1][None, :]
    tap_last = conv_taps[2][None, :]
    product = proj_c.astype(jnp.float32) * proj_x.astype(jnp.float32)
    before = passed_along(product[-2:], "sp", 1)
    padded = jnp.concatenate([before, product], axis=0)
    conv = tap_first * padded[:-2] + tap_middle * padded[1:-1] + tap_last * padded[2:]
    mixed = (proj_b.astype(jnp.float32) * conv).astype(jnp.bfloat16)
    grad_out_weight = lax.psum_scatter(
        lax.dot_general(
            grad_input, mixed, contract_first, preferred_element_type=jnp.float32
        ).astype(jnp.bfloat16),
        "sp",
        scatter_dimension=0,
        tiled=True,
    ).astype(jnp.float32)
    grad_mixed = jnp.dot(grad_input, out_weight, preferred_element_type=jnp.float32).astype(
        jnp.bfloat16
    )
    grad_b = (grad_mixed.astype(jnp.float32) * conv).astype(jnp.bfloat16)
    grad_conv = grad_mixed.astype(jnp.float32) * proj_b.astype(jnp.float32)
    after = passed_along(grad_conv[:2], "sp", -1)
    padded_back = jnp.concatenate([grad_conv, after], axis=0)
    grad_product = (
        tap_last * padded_back[:-2] + tap_middle * padded_back[1:-1] + tap_first * padded_back[2:]
    )
    grad_c = (grad_product * proj_x.astype(jnp.float32)).astype(jnp.bfloat16)
    grad_x = (grad_product * proj_c.astype(jnp.float32)).astype(jnp.bfloat16)
    return (
        gate_grad.astype(jnp.bfloat16)[None],
        up_grad.astype(jnp.bfloat16)[None],
        down_grad.astype(jnp.bfloat16)[None],
        grad_out_weight,
        grad_b,
        grad_c,
        grad_x,
    )


def solution(mesh):
    return jax.shard_map(
        on_device,
        mesh=mesh,
        in_specs=(
            P("sp", None),
            P(),
            P("sp", None),
            P("sp", None),
            P("sp", None),
            P("sp", "tp", None),
            P("sp", "tp", None),
            P("sp", "tp", None),
            P("sp", "tp"),
            P("sp", "tp"),
            P("sp", "tp"),
            P(None, "tp"),
            P(None, "tp"),
        ),
        out_specs=(
            P("sp", "tp", None),
            P("sp", "tp", None),
            P("sp", "tp", None),
            P("sp", "tp"),
            P("sp", "tp"),
            P("sp", "tp"),
            P("sp", "tp"),
        ),
        check_vma=False,
    )
```

profile of v0, /device:TPU:30, one launch (start us, length us, event | category | flops | bytes accessed | tf_op | source)
XLA Modules:
  0.0 287.3 jit_solution(17894055832276534300)
XLA Ops:
  7.2 0.0 copy-start
  7.2 0.0 all-gather.5.cloned.1.call-start
  7.2 0.8 broadcast_multiply_fusion
  8.1 0.8 copy.21
  8.9 0.1 eq.29
  9.0 0.1 eq.25
  9.1 1.4 fusion.3
  10.5 0.1 copy.20
  10.7 0.1 mul.161
  10.8 0.9 reduce-window.6
  11.7 0.2 slice_reduce_fusion
  11.9 0.1 fusion.31
  12.1 2.9 %scatter_custom_fusion.1 = s32[768]{0:T(1024)S(1)} fusion(s32[384]{0:T(512)S(1)} %fusion.39, s32[384]{0:T(512)S(1)} %iota.11, s32[]{:T(128)} %constant.15.clone.1), kind=kCustom, calls=%fused_computation.84 | custom fusion | bytes 3076 | tf_op jit(solution)/shard_map/scatter | solution.py:25
  15.0 2.9 %scatter_custom_fusion = s32[768]{0:T(1024)S(1)} fusion(s32[384]{0:T(512)S(1)} %fusion.39, s32[384]{0:T(512)S(1)} %broadcast.98, s32[]{:T(128)} %constant.15.clone.1), kind=kCustom, calls=%fused_computation.87 | custom fusion | bytes 3076 | tf_op jit(solution)/shard_map/scatter | solution.py:27
  18.0 0.1 broadcast_in_dim.54
  18.1 2.6 convert_divide_fusion
  20.7 4.2 %gather_fusion.2 = bf16[768,2048]{1,0:T(8,128)(2,1)} fusion(bf16[192,2048]{1,0:T(8,128)(2,1)S(1)} %get-tuple-element.14, s32[1024]{0:T(1024)S(1)} %get-tuple-element.21), kind=kCustom, calls=%fused_computation.2 | custom fusion | bytes 6294528 | tf_op jit(solution)/shard_map/gather | solution.py:60
  24.9 1.4 dynamic-slice_select_fusion
  26.4 23.8 %all_to_all.15 = bf16[8,96,512]{2,1,0:T(8,128)(2,1)} all-to-all(bf16[8,96,512]{2,1,0:T(8,128)(2,1)S(1)} %dynamic-slice_select_fusion), channel_id=1, replica_groups=mesh['sp'=8,'tp'=4] {'sp'}, dimensions={0} | all-to-all | bytes 1572864 | tf_op jit(solution)/shard_map/all_to_all | solution.py:74
  50.1 0.0 all-gather.5.cloned.1.call-update
  50.2 0.0 all-gather.3.cloned.1.call-start
  50.2 0.1 copy.23
  50.3 0.1 reshape.114
  50.5 5.0 %gather_fusion = f32[768]{0:T(1024)S(1)} fusion(f32[384]{0:T(512)S(1)} %reshape.114, s32[1024]{0:T(1024)S(1)} %get-tuple-element.22), kind=kCustom, calls=%fused_computation | custom fusion | bytes 9216 | tf_op jit(solution)/shard_map/gather | solution.py:63
  55.5 0.1 mul.163
  55.6 4.3 %gather_fusion.1 = bf16[768,2048]{1,0:T(8,128)(2,1)} fusion(bf16[192,2048]{1,0:T(8,128)(2,1)S(1)} %copy-done.1, s32[1024]{0:T(1024)S(1)} %get-tuple-element.21), kind=kCustom, calls=%fused_computation.1 | custom fusion | bytes 6294528 | tf_op jit(solution)/shard_map/gather | solution.py:63
  59.9 1.5 fusion.5
  61.3 23.4 %all_to_all.16 = bf16[8,96,512]{2,1,0:T(8,128)(2,1)} all-to-all(bf16[8,96,512]{2,1,0:T(8,128)(2,1)S(1)} %fusion.5), channel_id=1, replica_groups=mesh['sp'=8,'tp'=4] {'sp'}, dimensions={0} | all-to-all | bytes 1572864 | tf_op jit(solution)/shard_map/all_to_all | solution.py:75
  84.7 0.0 all-gather.3.cloned.1.call-update
  84.7 0.2 reduce-scatter.3.cloned.1.call-start
  85.0 0.0 all-gather.5.cloned.1.call-done
  85.0 0.0 copy-start.3
  85.0 4.2 %fusion.9 = f32[768,256]{1,0:T(8,128)} fusion(bf16[768,2048]{1,0:T(8,128)(2,1)} %bitcast.61, bf16[1,256,2048]{2,1,0:T(8,128)(2,1)} %param.18), kind=kOutput, calls=%fused_computation.25 | convolution fusion | flops 805306368 | bytes 4980736 | tf_op jit(solution)/shard_map/dot_general | solution.py:88
  89.2 1.9 fusion.12
  91.1 22.2 %all-gather.3.cloned.1.call-done = bf16[8,96,2048]{2,1,0:T(8,128)(2,1)} async-done(((bf16[8,96,512]{2,1,0:T(8,128)(2,1)}), bf16[8,96,2048]{2,1,0:T(8,128)(2,1)}) %all-gather.3.cloned.1.call-update) | async-done | bytes 3145744 | tf_op jit(solution)/shard_map/all_gather | solution.py:79
  113.4 3.9 %multiply_convert_fusion.2 = (bf16[768,256]{1,0:T(8,128)(2,1)S(1)}, bf16[768,256]{1,0:T(8,128)(2,1)S(1)}) fusion(f32[768,256]{1,0:T(8,128)} %fusion.9, f32[768,256]{1,0:T(8,128)} %fusion.12, bf16[768,2048]{1,0:T(8,128)(2,1)} %bitcast.65, bf16[1,256,2048]{2,1,0:T(8,128)(2,1)} %param.20), kind=kOutput, calls=%fused_computation.34 | convolution fusion | flops 807862272 | bytes 6553600 | tf_op jit(solution)/shard_map/dot_general | solution.py:90
  117.3 1.0 fusion.7
  118.3 0.5 copy-done.4
  118.8 2.7 add_convert_fusion
  121.5 0.0 reduce-scatter.3.cloned.1.call-update
  121.5 37.9 %reduce-scatter.3.cloned.1.call-done = bf16[8,96,512]{2,1,0:T(8,128)(2,1)} async-done(((bf16[8,96,2048]{2,1,0:T(8,128)(2,1)}), bf16[8,96,512]{2,1,0:T(8,128)(2,1)}) %reduce-scatter.3.cloned.1.call-update) | async-done | bytes 786448 | tf_op jit(solution)/shard_map/reduce_scatter | solution.py:111
  159.4 6.0 %all-to-all-start.2 = ((bf16[8,96,512]{2,1,0:T(8,128)(2,1)}), bf16[8,96,512]{2,1,0:T(8,128)(2,1)}, u32[]{:S(2)}, u32[]{:S(2)}) async-start(bf16[8,96,512]{2,1,0:T(8,128)(2,1)} %reduce-scatter.3.cloned.1.call-done), calls=%async_computation.3 | async-start | bytes 1572864 | tf_op jit(solution)/shard_map/all_to_all | solution.py:114
  165.5 0.7 copy-done.10
  166.2 1.3 collective-permute-start
  167.5 0.8 dynamic_slice.18
  168.3 14.8 %all-to-all-done.2 = bf16[8,96,512]{2,1,0:T(8,128)(2,1)} async-done(((bf16[8,96,512]{2,1,0:T(8,128)(2,1)}), bf16[8,96,512]{2,1,0:T(8,128)(2,1)}, u32[]{:S(2)}, u32[]{:S(2)}) %all-to-all-start.2) | async-done | bytes 786464 | tf_op jit(solution)/shard_map/all_to_all | solution.py:114
  183.1 3.3 %gather_fusion.3 = bf16[384,512]{1,0:T(8,128)(2,1)S(1)} fusion(bf16[768,512]{1,0:T(8,128)(2,1)} %bitcast.13, s32[1024]{0:T(1024)S(1)} %pad_clamp_fusion), kind=kCustom, calls=%fused_computation.3 | custom fusion | bytes 787968 | tf_op jit(solution)/shard_map/gather | solution.py:116
  186.5 1.4 reshape.119
  187.8 2.1 reduce_sum.41
  189.9 1.1 multiply_reduce_fusion
  191.0 6.8 %psum.7 = f32[192]{0:T(256)S(1)} all-reduce(f32[192]{0:T(256)S(1)} %multiply_reduce_fusion), channel_id=1, replica_groups=mesh['sp'=8,'tp'=4] {'tp'}, use_global_device_ids=true, to_apply=%region_9.10 | all-reduce | flops 192 | bytes 1536 | tf_op jit(solution)/shard_map/psum | solution.py:122
  197.8 1.2 add_convert_fusion.1
  199.1 7.7 %all_gather.11 = bf16[192,2048]{1,0:T(8,128)(2,1)S(1)} all-gather(bf16[192,512]{1,0:T(8,128)(2,1)S(1)} %add_convert_fusion.1), channel_id=1, replica_groups=mesh['sp'=8,'tp'=4] {'tp'}, dimensions={1}, use_global_device_ids=true | all-gather | bytes 983040 | tf_op jit(solution)/shard_map/all_gather | solution.py:128
  206.8 2.8 multiply_convert_fusion.5
  209.5 2.1 convolution_convert_fusion
  211.6 0.0 reduce-scatter.5.cloned.1.call-update
  211.7 4.0 %fusion = bf16[1,256,2048]{2,1,0:T(8,128)(2,1)} fusion(bf16[768,256]{1,0:T(8,128)(2,1)S(1)} %copy-done.9, bf16[768,2048]{1,0:T(8,128)(2,1)} %bitcast.62), kind=kOutput, calls=%fused_computation.11 | convolution fusion | flops 805830656 | bytes 4587520 | tf_op jit(solution)/shard_map/dot_general | solution.py:102
  215.8 2.0 fusion.2
  217.8 2.3 collective-permute-start.1
  220.1 2.0 fusion.1
  222.1 0.8 fusion.25
  222.9 0.7 fusion.26
  223.7 55.3 %reduce-scatter.5.cloned.1.call-done = bf16[256,512]{1,0:T(8,128)(2,1)} async-done(((bf16[2048,512]{1,0:T(8,128)(2,1)}), bf16[256,512]{1,0:T(8,128)(2,1)}) %reduce-scatter.5.cloned.1.call-update) | async-done | bytes 262160 | tf_op jit(solution)/shard_map/reduce_scatter | solution.py:137
  278.9 1.8 convert_element_type.119
  (55 shorter events, 0.3 us)
Async XLA Ops:
  7.2 199.6 %copy-start = (bf16[2048,512]{1,0:T(8,128)(2,1)S(1)}, bf16[2048,512]{1,0:T(8,128)(2,1)}, u32[]{:S(2)}) copy-start(bf16[2048,512]{1,0:T(8,128)(2,1)} %param.25) | copy-start | bytes 6291460
  7.2 77.8 %all-gather.5.cloned.1.call-start = ((), (), s32[]{:S(2)}) async-start(), calls=%async_computation.6 | async-start | bytes 3932160 | tf_op jit(solution)/shard_map/all_gather | solution.py:78
  24.9 25.3 %copy-start.15 = (f32[192,2]{0,1:T(2,128)S(1)}, f32[192,2]{0,1:T(2,128)}, u32[]{:S(2)}) copy-start(f32[192,2]{0,1:T(2,128)} %param.16) | copy-start | bytes 4612
  26.3 29.2 %copy-start.1 = (bf16[192,2048]{1,0:T(8,128)(2,1)S(1)}, bf16[192,2048]{1,0:T(8,128)(2,1)}, u32[]{:S(2)}) copy-start(bf16[192,2048]{1,0:T(8,128)(2,1)} %param.17) | copy-start | bytes 2359300
  50.2 63.2 %all-gather.3.cloned.1.call-start = ((), (), s32[]{:S(2)}) async-start(), calls=%async_computation.5 | async-start | bytes 3932160 | tf_op jit(solution)/shard_map/all_gather | solution.py:79
  84.7 74.7 %reduce-scatter.3.cloned.1.call-start = ((), (), s32[]{:S(2)}) async-start(), calls=%async_computation.7 | async-start | bytes 3932160 | tf_op jit(solution)/shard_map/reduce_scatter | solution.py:111
  85.0 4.2 %copy-start.3 = (bf16[1,256,2048]{2,1,0:T(8,128)(2,1)S(1)}, bf16[1,256,2048]{2,1,0:T(8,128)(2,1)}, u32[]{:S(2)}) copy-start(bf16[1,256,2048]{2,1,0:T(8,128)(2,1)} %param.19) | copy-start | bytes 3145732
  85.0 4.2 %copy-start.16 = (bf16[8,96,2048]{2,1,0:T(8,128)(2,1)S(1)}, bf16[8,96,2048]{2,1,0:T(8,128)(2,1)}, u32[]{:S(2)}) copy-start(bf16[8,96,2048]{2,1,0:T(8,128)(2,1)} %all-gather.5.cloned.1.call-done) | copy-start | bytes 9437188
  113.4 3.9 %copy-start.2 = (bf16[1,256,2048]{2,1,0:T(8,128)(2,1)S(1)}, bf16[1,256,2048]{2,1,0:T(8,128)(2,1)}, u32[]{:S(2)}) copy-start(bf16[1,256,2048]{2,1,0:T(8,128)(2,1)} %param.18) | copy-start | bytes 3145732
  117.3 1.0 copy-start.8
  117.3 1.0 copy-start.11
  117.3 1.5 copy-start.4
  121.5 43.9 %copy-start.5 = (bf16[192,512]{1,0:T(8,128)(2,1)S(1)}, bf16[192,512]{1,0:T(8,128)(2,1)}, u32[]{:S(2)}) copy-start(bf16[192,512]{1,0:T(8,128)(2,1)} %param.22) | copy-start | bytes 589828
  121.5 43.9 %copy-start.6 = (bf16[192,512]{1,0:T(8,128)(2,1)S(1)}, bf16[192,512]{1,0:T(8,128)(2,1)}, u32[]{:S(2)}) copy-start(bf16[192,512]{1,0:T(8,128)(2,1)} %param.23) | copy-start | bytes 589828
  121.5 46.8 %copy-start.14 = (f32[3,512]{1,0:T(4,128)S(1)}, f32[3,512]{1,0:T(4,128)}, u32[]{:S(2)}) copy-start(f32[3,512]{1,0:T(4,128)} %param.24) | copy-start | bytes 18436
  159.4 23.7 %all-to-all-start.2 = ((bf16[8,96,512]{2,1,0:T(8,128)(2,1)}), bf16[8,96,512]{2,1,0:T(8,128)(2,1)}, u32[]{:S(2)}, u32[]{:S(2)}) async-start(bf16[8,96,512]{2,1,0:T(8,128)(2,1)} %reduce-scatter.3.cloned.1.call-done), calls=%async_computation.3 | async-start | bytes 1572864 | tf_op jit(solution)/shard_map/all_to_all | solution.py:114
  165.4 113.5 %reduce-scatter.5.cloned.1.call-start = ((), (), s32[]{:S(2)}) async-start(), calls=%async_computation.8 | async-start | bytes 2359296 | tf_op jit(solution)/shard_map/reduce_scatter | solution.py:137
  165.5 0.8 copy-start.10
  166.2 40.5 %collective-permute-start = (f32[2,512]{1,0:T(2,128)S(1)}, f32[2,512]{1,0:T(2,128)S(1)}, u32[]{:S(2)}, u32[]{:S(2)}) collective-permute-start(f32[2,512]{1,0:T(2,128)S(1)} %slice.53), channel_id=1, source_target_pairs={{0,4},{4,8},{8,12},{12,16},{16,20},{20,24},{24,28},{1,5},{5,9},{9,... | collective-permute-start | bytes 12296 | tf_op jit(solution)/shard_map/ppermute | solution.py:12
  197.8 11.7 %copy-start.13 = (bf16[192,512]{1,0:T(8,128)(2,1)S(1)}, bf16[192,512]{1,0:T(8,128)(2,1)}, u32[]{:S(2)}) copy-start(bf16[192,512]{1,0:T(8,128)(2,1)} %param.21) | copy-start | bytes 589828
  209.5 2.1 copy-start.9
  211.7 4.0 %copy-start.18 = (bf16[8,96,2048]{2,1,0:T(8,128)(2,1)S(1)}, bf16[8,96,2048]{2,1,0:T(8,128)(2,1)}, u32[]{:S(2)}) copy-start(bf16[8,96,2048]{2,1,0:T(8,128)(2,1)} %all-gather.3.cloned.1.call-done) | copy-start | bytes 9437188
  211.7 4.0 %copy-start.19 = (f32[768,256]{1,0:T(8,128)S(1)}, f32[768,256]{1,0:T(8,128)}, u32[]{:S(2)}) copy-start(f32[768,256]{1,0:T(8,128)} %fusion.9) | copy-start | bytes 2359300
  211.7 4.0 %copy-start.20 = (f32[768,256]{1,0:T(8,128)S(1)}, f32[768,256]{1,0:T(8,128)}, u32[]{:S(2)}) copy-start(f32[768,256]{1,0:T(8,128)} %fusion.12) | copy-start | bytes 2359300
  215.7 4.4 %copy-start.12 = (bf16[768,256]{1,0:T(8,128)(2,1)S(1)}, bf16[768,256]{1,0:T(8,128)(2,1)}, u32[]{:S(2)}) copy-start(bf16[768,256]{1,0:T(8,128)(2,1)} %copy-done.11) | copy-start | bytes 1179652
  215.7 4.4 %copy-start.17 = (bf16[8,96,2048]{2,1,0:T(8,128)(2,1)S(1)}, bf16[8,96,2048]{2,1,0:T(8,128)(2,1)}, u32[]{:S(2)}) copy-start(bf16[8,96,2048]{2,1,0:T(8,128)(2,1)} %all-gather.5.cloned.1.call-done) | copy-start | bytes 9437188
  217.8 5.1 %copy-start.7 = (bf16[192,512]{1,0:T(8,128)(2,1)S(1)}, bf16[192,512]{1,0:T(8,128)(2,1)}, u32[]{:S(2)}) copy-start(bf16[192,512]{1,0:T(8,128)(2,1)} %param.23) | copy-start | bytes 589828
  217.8 4.3 %collective-permute-start.1 = (f32[2,512]{1,0:T(2,128)S(1)}, f32[2,512]{1,0:T(2,128)S(1)}, u32[]{:S(2)}, u32[]{:S(2)}) collective-permute-start(f32[2,512]{1,0:T(2,128)S(1)} %slice.56), channel_id=1, source_target_pairs={{4,0},{8,4},{12,8},{16,12},{20,16},{24,20},{28,24},{5,1},{9,5},{13... | collective-permute-start | bytes 12296 | tf_op jit(solution)/shard_map/ppermute | solution.py:12
Sparse Core Ops, SparseCore 0:
  50.3 28.4 all-gather.4
  84.8 28.4 all-gather.2
  121.6 37.7 reduce-scatter.2
  211.8 67.1 reduce-scatter.4
where the time goes:
time: 292 us; the launch traced here: 287 us
  waiting for transfers between devices  130 us (45%)
  blocking collectives  61.6 us (21%)
  local copies, waits for them, and re-layouts  28.1 us (10%)
  matrix products  26.6 us (9%)
  other arithmetic  16.6 us (6%)
  between operations  14.2 us (5%)
  starting transfers between devices  9.87 us (3%)
    reduce_scatter x1, waiting for transfers between devices, on_device(): lax.psum_scatter(lax.dot_general(grad_input, mixed, contract_first, prefe...  55.3 us
    reduce_scatter x1, waiting for transfers between devices, on_device(): lax.psum_scatter(partial_value.astype(jnp.bfloat16), 'tp', scatter_dimens...  37.9 us
    all_to_all x1, blocking collectives, on_device(): lax.all_to_all(rows_cut, 'sp', split_axis=0, concat_axis=0, tiled=True)  23.8 us
    all_to_all x1, blocking collectives, on_device(): lax.all_to_all(cots_cut, 'sp', split_axis=0, concat_axis=0, tiled=True)  23.4 us
    all_gather x1, waiting for transfers between devices, on_device(): lax.all_gather(cots_part, 'tp', axis=2, tiled=True)  22.2 us
    all_to_all x1, waiting for transfers between devices, on_device(): back = lax.all_to_all(summed, 'sp', split_axis=0, concat_axis=0, tiled=True)  14.8 us
    all_gather x1, blocking collectives, on_device(): grad_input = lax.all_gather(grad_cols, 'tp', axis=1, tiled=True)  7.69 us
    psum x1, blocking collectives, on_device(): row_total = lax.psum(local_total, 'tp')  6.82 us
  transfers between devices with their start and end apart: 7, of which 4 were waited for; matrix products, arithmetic and copies ran while one was open for 13% of the time, Pallas kernels for 0%

commit v1 on v0

v1 whole, which is shorter than its diff:
```python
import functools

import jax
import jax.numpy as jnp
from jax import lax
from jax.experimental import pallas as pl
from jax.experimental.pallas import tpu as pltpu
from jax.sharding import PartitionSpec as P

eps = 1e-06
MESH = pl.DeviceIdType.MESH
f32 = jnp.float32
bf16 = jnp.bfloat16

NT = (((1,), (1,)), ((), ()))
TN = (((0,), (0,)), ((), ()))


def dot(a, b, dims=(((1,), (0,)), ((), ()))):
    return lax.dot_general(a, b, dims, preferred_element_type=f32)


def kernel(
    dims,
    x_ref, gain_ref, ids_ref, rw_ref, cot_ref, wg_h, wu_h, wd_h, pb_ref, pc_ref, px_ref, taps_ref, ow_h,
    gg_h, gu_h, gd_h, gow_ref, gb_ref, gc_ref, gx_ref,
    wg, wu, wd, ow, perm, send, R, hid, ggp, gup, pown, pcs, pcr, ysnd, yrcv, bsnd, back,
    gn, gi, GI, MX, conv, gmix, halo_s, halo_r, tail_s, tail_r, ggv, guv, gdv,
    lsem, osem, own_sem, a_s, r_sem, f_s, f2_s, p_s, p_r, y_s, y_r, b_s, b_r,
    n_s, n_r, n2_s, m_s, m_r, m2_s, g_s, g_r, g2_s, g2_r, h_s, h_r,
):
    G, T, C, lo = dims
    Y = T // 2
    H = G // lo
    tok, D = x_ref.shape
    col = D // T
    DB = D // G
    half = tok // 2
    me = lax.axis_index("sp")
    tp = lax.axis_index("tp")
    y = tp // 2
    c = lax.rem(tp, 2)
    oc = 1 - c
    ptn = y * 2 + oc

    def ring(v):
        return lax.rem(v + G, G)

    def yk(k):
        return lax.rem(y + k, Y)

    def rc(src, dst, ss, rs, sp, t):
        return pltpu.make_async_remote_copy(
            src_ref=src, dst_ref=dst, send_sem=ss, recv_sem=rs,
            device_id={"sp": sp, "tp": t}, device_id_type=MESH,
        )

    def far(i):
        k = i - 1
        d = G // 2 + ((k + 1) // 2) * (1 - 2 * lax.rem(k + 2, 2))
        return jnp.where(i == 0, 0, d)

    def src_at(i):
        return ring(me - far(i))

    def dst_at(i):
        return ring(me + far(i))

    loads = [
        pltpu.make_async_copy(h, v, lsem.at[n])
        for n, (h, v) in enumerate(((wg_h, wg), (wu_h, wu), (wd_h, wd), (ow_h, ow)))
    ]
    for ld in loads:
        ld.start()

    barrier = pltpu.get_barrier_semaphore()

    def greet(d, _):
        pl.semaphore_signal(barrier, inc=1, device_id={"sp": ring(me + d), "tp": tp}, device_id_type=MESH)
        return 0

    lax.fori_loop(1, G, greet, 0)
    for k in range(1, Y):
        pl.semaphore_signal(barrier, inc=1, device_id={"sp": me, "tp": yk(k) * 2 + c}, device_id_type=MESH)
    pl.semaphore_signal(barrier, inc=1, device_id={"sp": me, "tp": ptn}, device_id_type=MESH)

    xf = x_ref[...].astype(f32)
    rm = jnp.sqrt(jnp.mean(xf * xf, axis=1, keepdims=True) + eps)
    my_cols = pl.ds(pl.multiple_of(tp * col, col), col)
    ncols = ((x_ref[:, my_cols].astype(f32) / rm) * gain_ref[:, my_cols]).astype(bf16)
    ids = ids_ref[...]
    expert = lax.broadcasted_iota(jnp.int32, (G, tok), 0)
    is0 = expert == ids[0:1]
    is1 = expert == ids[1:2]
    both = jnp.where(is0 | is1, 1.0, 0.0).astype(bf16)
    earlier = jnp.where(
        lax.broadcasted_iota(jnp.int32, (tok, tok), 0) < lax.broadcasted_iota(jnp.int32, (tok, tok), 1), 1.0, 0.0
    ).astype(bf16)
    rank = dot(both, earlier)
    slot0 = jnp.sum(jnp.where(is0, rank, 0.0), axis=0, keepdims=True) + ids[0:1].astype(f32) * C
    slot1 = jnp.sum(jnp.where(is1, rank, 0.0), axis=0, keepdims=True) + ids[1:2].astype(f32) * C
    place = lax.broadcasted_iota(jnp.int32, (G * C, tok), 0).astype(f32)
    at0 = place == slot0
    at1 = place == slot1
    perm[...] = jnp.where(at0 | at1, 1.0, 0.0).astype(bf16)
    wslot = jnp.sum(jnp.where(at0, rw_ref[0:1], 0.0) + jnp.where(at1, rw_ref[1:2], 0.0), axis=1, keepdims=True)
    send[:, 0] = dot(perm[...], ncols).astype(bf16).reshape(G, C, col)
    send[:, 1] = (dot(perm[...], cot_ref[:, my_cols]) * wslot).astype(bf16).reshape(G, C, col)

    halo_s[...] = pc_ref[tok - 8:, :].astype(f32) * px_ref[tok - 8:, :].astype(f32)

    pl.semaphore_wait(barrier, G - 1 + Y)

    halo = rc(halo_s, halo_r, h_s.at[0], h_r.at[0], ring(me + 1), tp)
    halo.start()
    own = pltpu.make_async_copy(send.at[me], R.at[tp, me], own_sem)
    own.start()

    def a_copy(i):
        e = dst_at(i)
        return rc(send.at[e], R.at[tp, me], a_s.at[e], r_sem.at[tp, me], e, tp)

    def issue_a(i, _):
        a_copy(i).start()
        return 0

    lax.fori_loop(1, G, issue_a, 0)

    product = pc_ref[...].astype(f32) * px_ref[...].astype(f32)
    halo.wait_recv()
    before = jnp.where(me > 0, halo_r[...], 0.0)
    padded = jnp.concatenate([before, product], axis=0)
    cv = taps_ref[0:1] * padded[6:6 + tok] + taps_ref[1:2] * padded[7:7 + tok] + taps_ref[2:3] * product
    conv[...] = cv
    MX[me] = (pb_ref[...].astype(f32) * cv).astype(bf16)
    hi, low = me // lo, lax.rem(me, lo)

    def m_copy(d):
        h2 = lax.rem(hi + d, H)
        return rc(MX.at[me], MX.at[me], m_s.at[h2], m_r.at[me], h2 * lo + low, tp)

    for ld in loads[:3]:
        ld.wait()
    own.wait()

    def r_wait(j, s):
        rc(R.at[j, s], R.at[j, s], own_sem, r_sem.at[j, s], me, ptn).wait_recv()

    def fwd(n, s):
        t = ptn if n == 0 else yk(n) * 2 + c
        return rc(R.at[tp, s], R.at[tp, s], f_s.at[n, s], r_sem.at[tp, s], me, t)

    def fwd2(k, s):
        j = yk(k) * 2 + c
        return rc(R.at[j, s], R.at[j, s], f2_s.at[k, s], r_sem.at[j, s], me, ptn)

    def p_copy(s):
        return rc(pcs.at[s], pcr.at[s], p_s.at[s], p_r.at[s], me, ptn)

    def y_copy(k, s):
        yo = yk(k)
        return rc(ysnd.at[s, yo], yrcv.at[s, y], y_s.at[yo, s], y_r.at[y, s], me, yo * 2 + c)

    def b_copy(s):
        return rc(bsnd.at[s], back.at[me], b_s.at[s], b_r.at[me], s, tp)

    def cols(j):
        return pl.ds(pl.multiple_of(j * col, col), col)

    def step(i, _):
        @pl.when(i < G)
        def _():
            s = src_at(i)

            @pl.when(i > 0)
            def _():
                r_wait(tp, s)

            for n in range(Y - 1, -1, -1):
                fwd(n, s).start()

        @pl.when((i >= 1) & (i < G + 1))
        def _():
            s = src_at(i - 1)
            for k in range(1, Y):
                r_wait(yk(k) * 2 + c, s)
                fwd2(k, s).start()

        @pl.when((i >= 2) & (i < G + 2))
        def _():
            s = src_at(i - 2)
            for yy in range(Y):
                r_wait(yy * 2 + oc, s)
            gate = jnp.zeros((C, wg.shape[0]), f32)
            up = gate
            gh = gate
            for j in range(T):
                rows = R[j, s, 0]
                cots = R[j, s, 1]
                cs = slice(j * col, (j + 1) * col)
                gate = gate + dot(rows, wg[:, cs], NT)
                up = up + dot(rows, wu[:, cs], NT)
                gh = gh + dot(cots, wd[:, cs], NT)
            sg = jax.nn.sigmoid(gate)
            hid[s] = (gate * sg * up).astype(bf16)
            a = (gh * up * sg * (1.0 + gate * (1.0 - sg))).astype(bf16)
            b = (gh * gate * sg).astype(bf16)
            ggp[s] = a
            gup[s] = b
            for yy in range(Y):
                jo = cols(yy * 2 + oc)
                pcs[s, yy] = (dot(a, wg[:, jo]) + dot(b, wu[:, jo])).astype(bf16)
            p_copy(s).start()
            for yy in range(Y):
                jm = cols(yy * 2 + c)
                pown[s, yy] = dot(a, wg[:, jm]) + dot(b, wu[:, jm])

        @pl.when((i >= 3) & (i < G + 3))
        def _():
            s = src_at(i - 3)
            p_copy(s).wait_recv()
            for k in range(1, Y):
                yo = yk(k)
                ysnd[s, yo] = (pown[s, yo] + pcr[s, yo].astype(f32)).astype(bf16)
                y_copy(k, s).start()

        @pl.when(i >= 4)
        def _():
            s = src_at(i - 4)
            total = pown[s, y] + pcr[s, y].astype(f32)
            for k in range(1, Y):
                yo = yk(k)
                rc(ysnd.at[s, yo], yrcv.at[s, yo], y_s.at[yo, s], y_r.at[yo, s], me, yo * 2 + c).wait_recv()
                total = total + yrcv[s, yo].astype(f32)

            @pl.when(i > 4)
            def _():
                bsnd[s] = total.astype(bf16)
                b_copy(s).start()

            @pl.when(i == 4)
            def _():
                back[me] = total.astype(bf16)

        return 0

    lax.fori_loop(0, G + 4, step, 0)

    for d in range(1, H):
        m_copy(d).start()

    def m2_copy(d, h2):
        lw = lax.rem(low + d, lo)
        s = h2 * lo + low
        return rc(MX.at[s], MX.at[s], m2_s.at[d, h2], m_r.at[s], hi * lo + lw, tp)

    for d in range(1, lo):
        m2_copy(d, hi).start()

    def wgrad(j, _):
        rows = R[j, :, 0].reshape(G * C, col)
        cots = R[j, :, 1].reshape(G * C, col)
        F = wg.shape[0]
        gdv[:, cols(j)] = dot(hid[...].reshape(G * C, F), cots, TN).astype(bf16)
        ggv[:, cols(j)] = dot(ggp[...].reshape(G * C, F), rows, TN).astype(bf16)
        guv[:, cols(j)] = dot(gup[...].reshape(G * C, F), rows, TN).astype(bf16)
        return 0

    lax.fori_loop(0, T, wgrad, 0)
    outs = [
        pltpu.make_async_copy(v, h, osem.at[n]) for n, (v, h) in enumerate(((ggv, gg_h), (guv, gu_h), (gdv, gd_h)))
    ]
    for o in outs:
        o.start()

    def back_wait(i, _):
        s = src_at(i)
        rc(back.at[s], back.at[s], b_s.at[s], b_r.at[s], s, tp).wait_recv()
        return 0

    lax.fori_loop(1, G, back_wait, 0)
    gn[tp] = dot(perm[...], back[...].reshape(G * C, col), TN).astype(bf16)

    def n_copy(n):
        t = ptn if n == 0 else yk(n) * 2 + c
        return rc(gn.at[tp], gn.at[tp], n_s.at[n], n_r.at[tp], me, t)

    def n2_copy(k):
        j = yk(k) * 2 + c
        return rc(gn.at[j], gn.at[j], n2_s.at[k], n_r.at[j], me, ptn)

    for n in range(Y - 1, -1, -1):
        n_copy(n).start()

    def m_recv(s):
        rc(MX.at[s], MX.at[s], m_s.at[0], m_r.at[s], me, ptn).wait_recv()

    for d in range(1, H):
        h2 = lax.rem(hi - d + H, H)
        m_recv(h2 * lo + low)
        for e in range(1, lo):
            m2_copy(e, h2).start()

    for k in range(1, Y):
        j = yk(k) * 2 + c
        rc(gn.at[j], gn.at[j], n2_s.at[k], n_r.at[j], me, ptn).wait_recv()
        n2_copy(k).start()
    for yy in range(Y):
        j = yy * 2 + oc
        rc(gn.at[j], gn.at[j], n_s.at[0], n_r.at[j], me, ptn).wait_recv()

    total = jnp.zeros((tok, 1), f32)
    inv = 1.0 / rm
    for j in range(T):
        cs = slice(j * col, (j + 1) * col)
        total = total + jnp.sum(
            (x_ref[:, cs].astype(f32) * inv) * (gain_ref[:, cs] * gn[j].astype(f32)), axis=1, keepdims=True
        )
    total = total * (1.0 / D)
    per = col // DB
    for j in range(T):
        cs = slice(j * col, (j + 1) * col)
        value = (
            cot_ref[:, cs].astype(f32)
            + (gain_ref[:, cs] * gn[j].astype(f32) - (x_ref[:, cs].astype(f32) * inv) * total) * inv
        ).astype(bf16)
        for q in range(per):
            gi[j * per + q] = value[:, q * DB:(q + 1) * DB].reshape(2, half, DB)

    def g_copy(i):
        s = dst_at(i)
        return rc(gi.at[s, c], GI.at[me, c], g_s.at[s], g_r.at[me], s, tp)

    def g2_copy(s):
        return rc(GI.at[s, c], GI.at[s, c], g2_s.at[s], g2_r.at[s], me, ptn)

    def issue_g(i, _):
        g_copy(i).start()
        return 0

    lax.fori_loop(1, G, issue_g, 0)

    loads[3].wait()

    acc = jnp.zeros((tok, ow.shape[1]), f32)
    for g in range(G):
        acc = acc + dot(gi[g].reshape(tok, DB), ow[g * DB:(g + 1) * DB, :])
    gm = acc.astype(bf16).astype(f32)
    gb_ref[...] = (gm * conv[...]).astype(bf16)
    gcv = gm * pb_ref[...].astype(f32)
    tail_s[...] = gcv[0:8]
    tail = rc(tail_s, tail_r, h_s.at[1], h_r.at[1], ring(me + G - 1), tp)
    tail.start()
    gmix[...] = gcv

    gow_ref[...] = dot(gi[me].reshape(tok, DB), MX[me], TN)

    for e in range(1, lo):
        lw = lax.rem(low + e, lo)
        for h2 in range(H):
            m_recv(h2 * lo + lw)

    tail.wait_recv()
    after = jnp.where(me < G - 1, tail_r[...], 0.0)
    pb2 = jnp.concatenate([gmix[...], after], axis=0)
    gp = taps_ref[2:3] * pb2[0:tok] + taps_ref[1:2] * pb2[1:1 + tok] + taps_ref[0:1] * pb2[2:2 + tok]
    gc_ref[...] = (gp * px_ref[...].astype(f32)).astype(bf16)
    gx_ref[...] = (gp * pc_ref[...].astype(f32)).astype(bf16)

    def finish(i, _):
        @pl.when(i < G)
        def _():
            s = src_at(i)
            rc(GI.at[s, c], GI.at[s, c], g_s.at[s], g_r.at[s], s, tp).wait_recv()
            g2_copy(s).start()

        @pl.when(i >= 2)
        def _():
            s = src_at(i - 1)
            rc(GI.at[s, oc], GI.at[s, oc], g2_s.at[s], g2_r.at[s], me, ptn).wait_recv()
            gow_ref[...] += dot(GI[s].reshape(tok, DB), MX[s], TN)

        return 0

    lax.fori_loop(1, G + 1, finish, 0)

    halo.wait_send()
    tail.wait_send()

    def drain(i, _):
        @pl.when(i > 0)
        def _():
            a_copy(i).wait_send()
            g_copy(i).wait_send()
            s = src_at(i)
            b_copy(s).wait_send()
            g2_copy(s).wait_send()

        s = src_at(i)
        for n in range(Y):
            fwd(n, s).wait_send()
        for k in range(1, Y):
            fwd2(k, s).wait_send()
            y_copy(k, s).wait_send()
        p_copy(s).wait_send()
        return 0

    lax.fori_loop(0, G, drain, 0)
    for d in range(1, H):
        m_copy(d).wait_send()
    for d in range(1, lo):
        for h2 in range(H):
            m2_copy(d, h2).wait_send()
    for n in range(Y):
        n_copy(n).wait_send()
    for k in range(1, Y):
        n2_copy(k).wait_send()
    for o in outs:
        o.wait()


def on_device(
    groups, slices,
    expert_input, norm_gain, expert_ids, route_weights, layer_cotangent,
    gate_weight, up_weight, down_weight, proj_b, proj_c, proj_x, conv_taps, out_weight,
):
    tok, D = expert_input.shape
    G, T = groups, slices
    Y = T // 2
    C = -(-(4 * tok // G) // 16) * 16
    lo = 1
    while lo * lo * 4 <= G:
        lo *= 2
    H = G // lo
    col = D // T
    DB = D // G
    F = gate_weight.shape[1]
    W = proj_b.shape[1]
    half = tok // 2
    vmem = pl.BlockSpec(memory_space=pltpu.VMEM)
    hbm = pl.BlockSpec(memory_space=pl.ANY)
    dma = pltpu.SemaphoreType.DMA
    V = pltpu.VMEM
    outs = pl.pallas_call(
        functools.partial(kernel, (G, T, C, lo)),
        out_shape=(
            jax.ShapeDtypeStruct((F, D), bf16),
            jax.ShapeDtypeStruct((F, D), bf16),
            jax.ShapeDtypeStruct((F, D), bf16),
            jax.ShapeDtypeStruct((DB, W), f32),
            jax.ShapeDtypeStruct((tok, W), bf16),
            jax.ShapeDtypeStruct((tok, W), bf16),
            jax.ShapeDtypeStruct((tok, W), bf16),
        ),
        in_specs=[vmem] * 5 + [hbm] * 3 + [vmem] * 4 + [hbm],
        out_specs=(hbm,) * 3 + (vmem,) * 4,
        scratch_shapes=[
            V((F, D), bf16), V((F, D), bf16), V((F, D), bf16), V((D, W), bf16),
            V((G * C, tok), bf16),
            V((G, 2, C, col), bf16),
            V((T, G, 2, C, col), bf16),
            V((G, C, F), bf16), V((G, C, F), bf16), V((G, C, F), bf16),
            V((G, Y, C, col), f32),
            V((G, Y, C, col), bf16), V((G, Y, C, col), bf16),
            V((G, Y, C, col), bf16), V((G, Y, C, col), bf16),
            V((G, C, col), bf16), V((G, C, col), bf16),
            V((T, tok, col), bf16),
            V((G, 2, half, DB), bf16), V((G, 2, half, DB), bf16),
            V((G, tok, W), bf16),
            V((tok, W), f32), V((tok, W), f32),
            V((8, W), f32), V((8, W), f32), V((8, W), f32), V((8, W), f32),
            V((F, D), bf16), V((F, D), bf16), V((F, D), bf16),
            dma((4,)), dma((3,)), dma(()),
            dma((G,)), dma((T, G)), dma((Y, G)), dma((Y, G)),
            dma((G,)), dma((G,)),
            dma((Y, G)), dma((Y, G)),
            dma((G,)), dma((G,)),
            dma((Y,)), dma((T,)), dma((Y,)),
            dma((H,)), dma((G,)), dma((lo, H)),
            dma((G,)), dma((G,)), dma((G,)), dma((G,)),
            dma((2,)), dma((2,)),
        ],
        compiler_params=pltpu.CompilerParams(
            collective_id=0, has_side_effects=True, vmem_limit_bytes=60 * 1024 * 1024
        ),
    )(
        expert_input, norm_gain[None, :], expert_ids.T, route_weights.T, layer_cotangent,
        gate_weight[0], up_weight[0], down_weight[0], proj_b, proj_c, proj_x, conv_taps, out_weight,
    )
    return (outs[0][None], outs[1][None], outs[2][None]) + tuple(outs[3:])


def solution(mesh):
    body = functools.partial(on_device, mesh.shape["sp"], mesh.shape["tp"])
    return jax.shard_map(
        body,
        mesh=mesh,
        in_specs=(
            P("sp", None), P(), P("sp", None), P("sp", None), P("sp", None),
            P("sp", "tp", None), P("sp", "tp", None), P("sp", "tp", None),
            P("sp", "tp"), P("sp", "tp"), P("sp", "tp"), P(None, "tp"), P(None, "tp"),
        ),
        out_specs=(
            P("sp", "tp", None), P("sp", "tp", None), P("sp", "tp", None),
            P("sp", "tp"), P("sp", "tp"), P("sp", "tp"), P("sp", "tp"),
        ),
        check_vma=False,
    )
```

time: 292 us -> 126 us (0.43); the launches traced: 287 us -> 126 us
  waiting for transfers between devices: 130 us -> 0 us
  Pallas kernels: 0 us -> 118 us
  blocking collectives: 61.6 us -> 0 us
  matrix products: 26.6 us -> 0 us
  local copies, waits for them, and re-layouts: 28.1 us -> 7.24 us
  other arithmetic: 16.6 us -> 0 us
  between operations: 14.2 us -> 0.67 us
  starting transfers between devices: 9.87 us -> 0 us
    pallas_call x0 -> x1, Pallas kernels: none -> 118 us  [on_device(): pl.pallas_call(functools.partial(kernel, (G, T, C, lo)), out_shape=(jax.S...]
    reduce_scatter x2 -> x0, waiting for transfers between devices: 93.2 us -> none  [the longest x1 55.3 us: on_device(): lax.psum_scatter(lax.dot_general(grad_input, mixed, contract_first, prefe...]
    all_to_all x2 -> x0, blocking collectives: 47.1 us -> none  [the longest x1 23.8 us: on_device(): lax.all_to_all(rows_cut, 'sp', split_axis=0, concat_axis=0, tiled=True)]
    dot_general x10 -> x0, matrix products: 26.6 us -> none  [the longest x1 4.22 us: on_device(): lax.dot_general(rows_flat, w_gate, contract_last, preferred_element_type=...]
    all_gather x2 -> x0, waiting for transfers between devices: 22.3 us -> none  [the longest x1 22.2 us: on_device(): lax.all_gather(cots_part, 'tp', axis=2, tiled=True)]
    gather x4 -> x0, local copies, waits for them, and re-layouts: 16.9 us -> none  [the longest x1 5.01 us: on_device(): route_weights.reshape(-1)[pair_of][:, None]]
    all_to_all x1 -> x0, waiting for transfers between devices: 14.8 us -> none  [on_device(): back = lax.all_to_all(summed, 'sp', split_axis=0, concat_axis=0, tiled=True)]
    all_gather x1 -> x0, blocking collectives: 7.69 us -> none  [on_device(): grad_input = lax.all_gather(grad_cols, 'tp', axis=1, tiled=True)]
  transfers between devices with their start and end apart: 7 -> 0, of which waited for: 4 -> 0; matrix products, arithmetic and copies ran while one was open for 13% -> 0% of each run, Pallas kernels for 0% -> 0%
where the time goes in v1:
time: 126 us
  Pallas kernels  118 us (94%)
  local copies, waits for them, and re-layouts  7.24 us (6%)
    pallas_call x1, Pallas kernels, on_device(): pl.pallas_call(functools.partial(kernel, (G, T, C, lo)), out_shape=(jax.S...  118 us
    unnamed x19, local copies, waits for them, and re-layouts  7.24 us

profile of v1, /device:TPU:30, one launch (start us, length us, event | category | flops | bytes accessed | tf_op | source)
XLA Modules:
  0.0 125.6 jit_solution(14481802829842494162)
XLA Ops:
  0.6 117.7 %shard_map.180 = (bf16[256,2048]{1,0:T(8,128)(2,1)}, bf16[256,2048]{1,0:T(8,128)(2,1)}, bf16[256,2048]{1,0:T(8,128)(2,1)}, f32[256,512]{1,0:T(8,128)}, bf16[192,...) custom-call(bf16[192,2048]{1,0:T(8,128)(2,1)} %x_ref.1, f32[1,2048]{1,0:T(1,128)} %bitcast.15, ...), custom_call_target="tpu_custom_call" | custom-call | tf_op jit(solution)/shard_map/pallas_call | solution.py:444
  118.3 0.0 copy-start.1
  118.3 0.0 copy-start
  118.3 2.5 %copy.27 = bf16[1,256,2048]{2,1,0:T(8,128)(2,1)} copy(bf16[1,256,2048]{2,1,0:T(8,128)(2,1)} %bitcast.14) | data formatting | bytes 2097152
  120.8 0.0 copy-done.1
  120.8 0.0 copy-start.2
  120.8 0.0 copy-start.5
  120.8 1.0 copy.28
  121.7 0.0 copy-done
  121.8 0.0 copy-start.4
  121.8 0.0 copy-start.3
  121.8 1.0 copy.29
  122.7 0.0 copy-done.2
  122.7 0.8 copy.30
  123.5 0.0 copy-done.5
  123.5 0.7 copy.31
  124.2 0.0 copy-done.4
  124.2 0.7 copy.32
  124.9 0.0 copy-done.3
  124.9 0.7 copy.33
Async XLA Ops:
  118.3 2.5 %copy-start.1 = (bf16[256,2048]{1,0:T(8,128)(2,1)S(1)}, bf16[256,2048]{1,0:T(8,128)(2,1)}, u32[]{:S(2)}) copy-start(bf16[256,2048]{1,0:T(8,128)(2,1)} %get-tuple-element.15) | copy-start | bytes 3145732
  118.3 3.4 %copy-start = (bf16[256,2048]{1,0:T(8,128)(2,1)S(1)}, bf16[256,2048]{1,0:T(8,128)(2,1)}, u32[]{:S(2)}) copy-start(bf16[256,2048]{1,0:T(8,128)(2,1)} %get-tuple-element.16) | copy-start | bytes 3145732
  120.8 2.0 %copy-start.2 = (f32[256,512]{1,0:T(8,128)S(1)}, f32[256,512]{1,0:T(8,128)}, u32[]{:S(2)}) copy-start(f32[256,512]{1,0:T(8,128)} %get-tuple-element.31) | copy-start | bytes 1572868
  120.8 2.7 %copy-start.5 = (bf16[192,512]{1,0:T(8,128)(2,1)S(1)}, bf16[192,512]{1,0:T(8,128)(2,1)}, u32[]{:S(2)}) copy-start(bf16[192,512]{1,0:T(8,128)(2,1)} %get-tuple-element.32) | copy-start | bytes 589828
  121.8 2.5 %copy-start.4 = (bf16[192,512]{1,0:T(8,128)(2,1)S(1)}, bf16[192,512]{1,0:T(8,128)(2,1)}, u32[]{:S(2)}) copy-start(bf16[192,512]{1,0:T(8,128)(2,1)} %get-tuple-element.33) | copy-start | bytes 589828
  121.8 3.1 %copy-start.3 = (bf16[192,512]{1,0:T(8,128)(2,1)S(1)}, bf16[192,512]{1,0:T(8,128)(2,1)}, u32[]{:S(2)}) copy-start(bf16[192,512]{1,0:T(8,128)(2,1)} %get-tuple-element.34) | copy-start | bytes 589828

commit v2 on v1

--- a/solution.py
+++ b/solution.py
@@ -35,6 +35,7 @@
     tok, D = x_ref.shape
     col = D // T
     DB = D // G
+    EARLY = min(2, H - 1)
     half = tok // 2
     me = lax.axis_index("sp")
     tp = lax.axis_index("tp")
@@ -135,9 +136,40 @@
     MX[me] = (pb_ref[...].astype(f32) * cv).astype(bf16)
     hi, low = me // lo, lax.rem(me, lo)
 
-    def m_copy(d):
-        h2 = lax.rem(hi + d, H)
-        return rc(MX.at[me], MX.at[me], m_s.at[h2], m_r.at[me], h2 * lo + low, tp)
+    def m_hop(h, way):
+        s = h * lo + low
+        to = lax.rem(hi + way + H, H)
+        return rc(MX.at[s], MX.at[s], m_s.at[h, (way + 1) // 2], m_r.at[s], to * lo + low, tp)
+
+    def m_start(h):
+        @pl.when((h >= 0) & (h <= hi) & (hi < H - 1))
+        def _():
+            m_hop(h, 1).start()
+
+        @pl.when((h < H) & (h >= hi) & (hi > 0))
+        def _():
+            m_hop(h, -1).start()
+
+    def m_arrive(h):
+        @pl.when((h >= 0) & (h < H))
+        def _():
+            m_recv(h * lo + low)
+            m_start(h)
+            for e in range(1, lo):
+                m2_copy(e, h).start()
+
+    def m_recv(s):
+        rc(MX.at[s], MX.at[s], own_sem, m_r.at[s], me, ptn).wait_recv()
+
+    m_start(hi)
+
+    def m2_copy(d, h2):
+        lw = lax.rem(low + d, lo)
+        s = h2 * lo + low
+        return rc(MX.at[s], MX.at[s], m2_s.at[d, h2], m_r.at[s], hi * lo + lw, tp)
+
+    for d in range(1, lo):
+        m2_copy(d, hi).start()
 
     for ld in loads[:3]:
         ld.wait()
@@ -168,6 +200,12 @@
         return pl.ds(pl.multiple_of(j * col, col), col)
 
     def step(i, _):
+        for d in range(1, EARLY + 1):
+            @pl.when(i == G + 2 * d - 2)
+            def _():
+                m_arrive(hi - d)
+                m_arrive(hi + d)
+
         @pl.when(i < G)
         def _():
             s = src_at(i)
@@ -246,17 +284,6 @@
 
     lax.fori_loop(0, G + 4, step, 0)
 
-    for d in range(1, H):
-        m_copy(d).start()
-
-    def m2_copy(d, h2):
-        lw = lax.rem(low + d, lo)
-        s = h2 * lo + low
-        return rc(MX.at[s], MX.at[s], m2_s.at[d, h2], m_r.at[s], hi * lo + lw, tp)
-
-    for d in range(1, lo):
-        m2_copy(d, hi).start()
-
     def wgrad(j, _):
         rows = R[j, :, 0].reshape(G * C, col)
         cots = R[j, :, 1].reshape(G * C, col)
@@ -273,6 +300,10 @@
     for o in outs:
         o.start()
 
+    for d in range(EARLY + 1, H):
+        m_arrive(hi - d)
+        m_arrive(hi + d)
+
     def back_wait(i, _):
         s = src_at(i)
         rc(back.at[s], back.at[s], b_s.at[s], b_r.at[s], s, tp).wait_recv()
@@ -291,15 +322,6 @@
 
     for n in range(Y - 1, -1, -1):
         n_copy(n).start()
-
-    def m_recv(s):
-        rc(MX.at[s], MX.at[s], m_s.at[0], m_r.at[s], me, ptn).wait_recv()
-
-    for d in range(1, H):
-        h2 = lax.rem(hi - d + H, H)
-        m_recv(h2 * lo + low)
-        for e in range(1, lo):
-            m2_copy(e, h2).start()
 
     for k in range(1, Y):
         j = yk(k) * 2 + c
@@ -406,8 +428,15 @@
         return 0
 
     lax.fori_loop(0, G, drain, 0)
-    for d in range(1, H):
-        m_copy(d).wait_send()
+    for h in range(H):
+        @pl.when((h <= hi) & (hi < H - 1))
+        def _():
+            m_hop(h, 1).wait_send()
+
+        @pl.when((h >= hi) & (hi > 0))
+        def _():
+            m_hop(h, -1).wait_send()
+
     for d in range(1, lo):
         for h2 in range(H):
             m2_copy(d, h2).wait_send()
@@ -415,6 +444,27 @@
         n_copy(n).wait_send()
     for k in range(1, Y):
         n2_copy(k).wait_send()
+    for o in outs:
+        o.wait()
+
+
+PIECES = 2
+
+
+def hand_over(*refs):
+    srcs, dsts, bufs, (i_s, o_s) = refs[:7], refs[7:14], refs[14:21], refs[21:]
+    ins, outs = [], []
+    for n in range(7):
+        rows = srcs[n].shape[0] // PIECES
+        for p in range(PIECES):
+            part = pl.ds(p * rows, rows)
+            ins.append(pltpu.make_async_copy(srcs[n].at[part], bufs[n].at[part], i_s.at[n, p]))
+            outs.append(pltpu.make_async_copy(bufs[n].at[part], dsts[n].at[part], o_s.at[n, p]))
+    for a in ins:
+        a.start()
+    for a, o in zip(ins, outs):
+        a.wait()
+        o.start()
     for o in outs:
         o.wait()
 
@@ -476,7 +526,7 @@
             dma((Y, G)), dma((Y, G)),
             dma((G,)), dma((G,)),
             dma((Y,)), dma((T,)), dma((Y,)),
-            dma((H,)), dma((G,)), dma((lo, H)),
+            dma((H, 2)), dma((G,)), dma((lo, H)),
             dma((G,)), dma((G,)), dma((G,)), dma((G,)),
             dma((2,)), dma((2,)),
         ],

time: 126 us -> 116 us (0.921); the launches traced: 126 us -> 114 us
  Pallas kernels: 118 us -> 106 us
    pallas_call x1, Pallas kernels: 118 us -> 106 us  [on_device(): pl.pallas_call(functools.partial(kernel, (G, T, C, lo)), out_shape=(jax.S...]
where the time goes in v2:
time: 116 us; the launch traced here: 114 us
  Pallas kernels  106 us (91%)
  local copies, waits for them, and re-layouts  7.24 us (6%)
    pallas_call x1, Pallas kernels, on_device(): pl.pallas_call(functools.partial(kernel, (G, T, C, lo)), out_shape=(jax.S...  106 us
    unnamed x19, local copies, waits for them, and re-layouts  7.24 us

profile of v2, /device:TPU:30, one launch (start us, length us, event | category | flops | bytes accessed | tf_op | source)
XLA Modules:
  0.0 114.1 jit_solution(1654652052593192750)
XLA Ops:
  0.6 106.2 %shard_map.180 = (bf16[256,2048]{1,0:T(8,128)(2,1)}, bf16[256,2048]{1,0:T(8,128)(2,1)}, bf16[256,2048]{1,0:T(8,128)(2,1)}, f32[256,512]{1,0:T(8,128)}, bf16[192,...) custom-call(bf16[192,2048]{1,0:T(8,128)(2,1)} %x_ref.1, f32[1,2048]{1,0:T(1,128)} %bitcast.15, ...), custom_call_target="tpu_custom_call" | custom-call | tf_op jit(solution)/shard_map/pallas_call | solution.py:494
  106.8 0.0 copy-start.1
  106.8 0.0 copy-start
  106.8 2.5 %copy.27 = bf16[1,256,2048]{2,1,0:T(8,128)(2,1)} copy(bf16[1,256,2048]{2,1,0:T(8,128)(2,1)} %bitcast.14) | data formatting | bytes 2097152
  109.3 0.0 copy-done.1
  109.3 0.0 copy-start.2
  109.3 0.0 copy-start.5
  109.3 1.0 copy.28
  110.3 0.0 copy-done
  110.3 0.0 copy-start.4
  110.3 0.0 copy-start.3
  110.3 1.0 copy.29
  111.2 0.0 copy-done.2
  111.2 0.8 copy.30
  112.0 0.0 copy-done.5
  112.0 0.7 copy.31
  112.7 0.0 copy-done.4
  112.7 0.7 copy.32
  113.4 0.0 copy-done.3
  113.4 0.7 copy.33
Async XLA Ops:
  106.8 2.5 %copy-start.1 = (bf16[256,2048]{1,0:T(8,128)(2,1)S(1)}, bf16[256,2048]{1,0:T(8,128)(2,1)}, u32[]{:S(2)}) copy-start(bf16[256,2048]{1,0:T(8,128)(2,1)} %get-tuple-element.15) | copy-start | bytes 3145732
  106.8 3.4 %copy-start = (bf16[256,2048]{1,0:T(8,128)(2,1)S(1)}, bf16[256,2048]{1,0:T(8,128)(2,1)}, u32[]{:S(2)}) copy-start(bf16[256,2048]{1,0:T(8,128)(2,1)} %get-tuple-element.16) | copy-start | bytes 3145732
  109.3 2.0 %copy-start.2 = (f32[256,512]{1,0:T(8,128)S(1)}, f32[256,512]{1,0:T(8,128)}, u32[]{:S(2)}) copy-start(f32[256,512]{1,0:T(8,128)} %get-tuple-element.31) | copy-start | bytes 1572868
  109.3 2.7 %copy-start.5 = (bf16[192,512]{1,0:T(8,128)(2,1)S(1)}, bf16[192,512]{1,0:T(8,128)(2,1)}, u32[]{:S(2)}) copy-start(bf16[192,512]{1,0:T(8,128)(2,1)} %get-tuple-element.32) | copy-start | bytes 589828
  110.3 2.5 %copy-start.4 = (bf16[192,512]{1,0:T(8,128)(2,1)S(1)}, bf16[192,512]{1,0:T(8,128)(2,1)}, u32[]{:S(2)}) copy-start(bf16[192,512]{1,0:T(8,128)(2,1)} %get-tuple-element.33) | copy-start | bytes 589828
  110.3 3.1 %copy-start.3 = (bf16[192,512]{1,0:T(8,128)(2,1)S(1)}, bf16[192,512]{1,0:T(8,128)(2,1)}, u32[]{:S(2)}) copy-start(bf16[192,512]{1,0:T(8,128)(2,1)} %get-tuple-element.34) | copy-start | bytes 589828
